TPU v7x, 512 devices: a 4x2x32 block of a 4x8x32 slice. The times are simulated.
512 devices in a mesh: grp: 2 (over y), sp: 32 (over z), tp: 8 (over x, core).
Axes of the slice: x: 4, y: 2, z: 32, core: 2. Of those that a mesh axis runs over, the one named last changes fastest.
The devices are a block of a 4x8x32 slice.
Arguments:
- tokens: bfloat16 [24576, 2048], P(('grp', 'sp'), 'tp'), parts along dimension 0, may hold values from -6 to 6
- norm_gain: float32 [2048], replicated, may hold values from 0.1 to 1.9
- qk_gain: float32 [4, 64], replicated, may hold values from 0.7 to 5.5
- w_query_window: bfloat16 [2048, 1024], P('sp', 'tp'), may hold values from -1 to 1
- w_key_window: bfloat16 [2048, 512], P('sp', 'tp'), may hold values from -1 to 1
- w_value_window: bfloat16 [2048, 512], P('sp', 'tp'), may hold values from -0.125 to 0.125
- sink_logits: float32 [16], P('tp'), may hold values from 0 to 5
- w_query_forget: bfloat16 [2048, 1024], P('sp', 'tp'), may hold values from -1 to 1
- w_key_forget: bfloat16 [2048, 1024], P('sp', 'tp'), may hold values from -1 to 1
- w_value_forget: bfloat16 [2048, 1024], P('sp', 'tp'), may hold values from -0.125 to 0.125
- gate_cum: float32 [24576, 16], P(('grp', 'sp'), 'tp'), parts along dimension 0, as said below
- w_merge: bfloat16 [2048, 2, 2048], P('sp', None, 'tp'), may hold values from -0.125 to 0.125
- w_branch: bfloat16 [2, 1024, 2048], P(None, 'sp', 'tp'), may hold values from -0.8984375 to 0.8984375
Outputs:
- mixed: bfloat16 [24576, 2048], P(('grp', 'sp'), 'tp'), parts along dimension 0
There are 2 independent parts, one for each index of `grp`. A program takes and returns all parts, laid end to end along the dimension named above; an argument that names none is the same for every part. Nothing has to cross between parts.
Inputs may be any that keep to these rules, and one draw needn't show every extreme that they name: `gate_cum`: along positions each head's values never rise.
All inputs are finite; a program needn't handle non-finite values.
Results may differ from a plain program's by a relative error of at most 0.012.
Values may be sent and summed in bfloat16 or wider, within the bound.
A program may use at most 64 MiB of HBM per device.

v0:
```python
import math
import jax
import jax.numpy as jnp
from jax import lax
from jax.sharding import PartitionSpec as P

HEAD = 64
WINDOW = 128
epsilon = 1e-06
big_negative = -1e30


def sent_together(arrays, axis, dim, along):
    widths = [a.shape[along] for a in arrays]
    both = jnp.concatenate(arrays, axis=along)
    filled = lax.all_gather(both, axis, axis=dim, tiled=True)
    return tuple(jnp.split(filled, [sum(widths[:k]) for k in range(1, len(widths))], axis=along))


def in_order(tiles, dim):
    dims = list(tiles.shape[1:])
    dims[dim] *= tiles.shape[0]
    return jnp.moveaxis(tiles, 0, dim).reshape(dims)


def sent_to_all(value, axis):
    size = lax.axis_size(axis)
    return lax.all_to_all(
        jnp.broadcast_to(value[None], (size, *value.shape)), axis, 0, 0, tiled=True
    )


def gather_directly(value, axis, dim):
    return in_order(sent_to_all(value, axis), dim)


def from_behind(value, axis, by):
    size = lax.axis_size(axis)
    pairs = [(i, i + by) for i in range(size) if 0 <= i + by < size]
    return lax.ppermute(value, axis, pairs)


def head_norm(raw, gain, head_count):
    split = raw.reshape(raw.shape[0], head_count, -1)
    scaled = split * lax.rsqrt(jnp.mean(split * split, axis=-1, keepdims=True) + epsilon) * gain
    return scaled.astype(jnp.bfloat16)


def window_attend(queries, keys_ext, values_ext, sink_rows, first_pos):
    row_count, head_count, head_size = queries.shape
    group_count = keys_ext.shape[1]
    span_rows = WINDOW // 2
    block_count = row_count // span_rows
    query_blocks = queries.reshape(
        block_count, span_rows, group_count, head_count // group_count, head_size
    )
    key_blocks = jnp.concatenate(
        [
            keys_ext[lag_index * span_rows : lag_index * span_rows + row_count].reshape(
                block_count, span_rows, group_count, head_size
            )
            for lag_index in range(3)
        ],
        axis=1,
    )
    value_blocks = jnp.concatenate(
        [
            values_ext[lag_index * span_rows : lag_index * span_rows + row_count].reshape(
                block_count, span_rows, group_count, head_size
            )
            for lag_index in range(3)
        ],
        axis=1,
    )
    scores = jnp.einsum(
        "nqgrd,nkgd->ngrqk", query_blocks, key_blocks, preferred_element_type=jnp.float32
    ) * head_size ** (-0.5)
    distance = WINDOW + jnp.arange(span_rows)[:, None] - jnp.arange(3 * span_rows)[None, :]
    key_pos = (
        first_pos
        - WINDOW
        + jnp.arange(block_count)[:, None] * span_rows
        + jnp.arange(3 * span_rows)[None, :]
    )
    is_valid = ((distance >= 0) & (distance < WINDOW))[None] & (key_pos >= 0)[:, None, :]
    is_valid = is_valid[:, None, None]
    sink_grid = sink_rows.reshape(1, group_count, head_count // group_count, 1)
    row_max = jnp.maximum(jnp.max(jnp.where(is_valid, scores, big_negative), axis=-1), sink_grid)
    weights = jnp.where(is_valid, jnp.exp(scores - row_max[..., None]), 0.0)
    row_total = jnp.sum(weights, axis=-1) + jnp.exp(sink_grid - row_max)
    prob_rows = (weights / row_total[..., None]).astype(jnp.bfloat16)
    mixed_sum = jnp.einsum(
        "ngrqk,nkgd->nqgrd", prob_rows, value_blocks, preferred_element_type=jnp.float32
    )
    return mixed_sum.reshape(row_count, head_count * head_size).astype(jnp.bfloat16)


def forget_groups(groups, keys, values, gates):
    head_count, head_size = (keys.shape[1], keys.shape[2])
    gates_all = lax.all_gather(gates, "sp", axis=0, tiled=True)

    def absorber(queries, query_gate, query_pos):

        def absorb(running, block):
            row_max, row_total, mixed_sum = running
            key_rows, value_rows, key_gate, key_pos = block
            scores = jnp.einsum(
                "qhd,khd->hqk", queries, key_rows, preferred_element_type=jnp.float32
            ) * head_size ** (-0.5)
            scores = scores + query_gate.T[:, :, None] - key_gate.T[:, None, :]
            is_valid = (query_pos[:, None] >= key_pos[None, :])[None]
            new_max = jnp.maximum(
                row_max, jnp.max(jnp.where(is_valid, scores, big_negative), axis=-1)
            )
            weights = jnp.where(is_valid, jnp.exp(scores - new_max[..., None]), 0.0)
            shrink = jnp.exp(row_max - new_max)
            row_total = row_total * shrink + jnp.sum(weights, axis=-1)
            mixed_sum = mixed_sum * shrink.T[:, :, None] + jnp.einsum(
                "hqk,khd->qhd",
                weights.astype(jnp.bfloat16),
                value_rows,
                preferred_element_type=jnp.float32,
            )
            return ((new_max, row_total, mixed_sum), None)

        return absorb

    initial = tuple(
        (
            (
                jnp.full((head_count, group[0].shape[0]), big_negative, jnp.float32),
                jnp.zeros((head_count, group[0].shape[0]), jnp.float32),
                jnp.zeros((group[0].shape[0], head_count, head_size), jnp.float32),
            )
            for group in groups
        )
    )
    first_row = jnp.int32(0)
    key_rows, value_rows = sent_together((keys, values), "sp", 0, 1)
    piece_rows = key_rows.shape[0]
    sub_rows = math.gcd(piece_rows, 2048)
    turns = piece_rows // sub_rows
    key_gate = gates_all
    key_pos = jnp.arange(piece_rows)
    blocks = (
        key_rows.reshape(turns, sub_rows, head_count, head_size),
        value_rows.reshape(turns, sub_rows, head_count, head_size),
        key_gate.reshape(turns, sub_rows, head_count),
        key_pos.reshape(turns, sub_rows),
    )
    updated = []
    for (queries, query_gate, query_pos), state in zip(groups, initial):
        absorb = absorber(queries, query_gate, query_pos)

        def advance(current):
            return lax.scan(absorb, current, blocks)[0]

        def keep(current):
            return current

        updated.append(lax.cond(first_row <= query_pos[-1], advance, keep, state))
    finals = tuple(updated)
    return [
        (mixed_sum / row_total.T[:, :, None])
        .reshape(mixed_sum.shape[0], head_count * head_size)
        .astype(jnp.bfloat16)
        for row_max, row_total, mixed_sum in finals
    ]


def on_device(
    tokens,
    norm_gain,
    qk_gain,
    w_query_window,
    w_key_window,
    w_value_window,
    sink_logits,
    w_query_forget,
    w_key_forget,
    w_value_forget,
    gate_cum,
    w_merge,
    w_branch,
):
    row_count = tokens.shape[0]
    row_offset = lax.axis_index("sp") * row_count
    gathered = gather_directly(tokens, "tp", 1)
    as_float = gathered.astype(jnp.float32)
    normed = (
        as_float
        * lax.rsqrt(jnp.mean(as_float * as_float, axis=-1, keepdims=True) + epsilon)
        * norm_gain
    ).astype(jnp.bfloat16)
    merge_flat = w_merge.reshape(w_merge.shape[0], -1)
    pieces = sent_together(
        (
            w_query_window,
            w_key_window,
            w_value_window,
            w_query_forget,
            w_key_forget,
            w_value_forget,
            merge_flat,
        ),
        "sp",
        0,
        1,
    )
    projected = tuple(
        (jnp.dot(normed, weight_rows, preferred_element_type=jnp.float32) for weight_rows in pieces)
    )
    query_heads = w_query_window.shape[1] // HEAD
    group_heads = w_key_window.shape[1] // HEAD
    window_query = head_norm(projected[0], qk_gain[0], query_heads)
    window_key = head_norm(projected[1], qk_gain[1], group_heads)
    window_value = projected[2].astype(jnp.bfloat16).reshape(row_count, group_heads, HEAD)
    prev_key, prev_value = from_behind(
        (window_key[row_count - WINDOW :], window_value[row_count - WINDOW :]), "sp", 1
    )
    window_out = window_attend(
        window_query,
        jnp.concatenate([prev_key, window_key], axis=0),
        jnp.concatenate([prev_value, window_value], axis=0),
        sink_logits,
        row_offset,
    )
    forget_query = head_norm(projected[3], qk_gain[2], query_heads)
    forget_key = head_norm(projected[4], qk_gain[3], query_heads)
    forget_value = projected[5].astype(jnp.bfloat16).reshape(row_count, query_heads, HEAD)
    own_pos = row_offset + jnp.arange(row_count)
    forget_out = forget_groups(
        [(forget_query, gate_cum, own_pos)], forget_key, forget_value, gate_cum
    )[0]
    channel_count = w_merge.shape[2]
    merge_gate = jax.nn.sigmoid(projected[6]).reshape(row_count, 2, channel_count)
    branch_full = lax.all_gather(w_branch, "sp", axis=1, tiled=True)
    head_stack = jnp.stack([window_out, forget_out], axis=1)
    weight_rows = branch_full
    projection = jnp.einsum(
        "uxa,xag->uxg",
        gather_directly(head_stack, "tp", 2),
        weight_rows,
        preferred_element_type=jnp.float32,
    )
    return (merge_gate[:, 0] * projection[:, 0] + merge_gate[:, 1] * projection[:, 1]).astype(
        jnp.bfloat16
    )


def solution(mesh):
    return jax.shard_map(
        on_device,
        mesh=mesh,
        in_specs=(
            P(("grp", "sp"), "tp"),
            P(),
            P(),
            P("sp", "tp"),
            P("sp", "tp"),
            P("sp", "tp"),
            P("tp"),
            P("sp", "tp"),
            P("sp", "tp"),
            P("sp", "tp"),
            P(("grp", "sp"), "tp"),
            P("sp", None, "tp"),
            P(None, "sp", "tp"),
        ),
        out_specs=P(("grp", "sp"), "tp"),
        check_vma=False,
    )
```

profile of v0, /device:TPU:34, one launch (start us, length us, event | category | flops | bytes accessed | tf_op | source)
XLA Modules:
  0.0 458.4 jit_solution(7849762737389114048)
XLA Ops:
  6.6 0.9 copy.129
  7.4 1.6 concatenate.18
  9.0 2.2 broadcast_in_dim.89
  11.2 43.9 %all-to-all-start = ((bf16[8,384,256]{2,1,0:T(8,128)(2,1)}), bf16[8,384,256]{2,1,0:T(8,128)(2,1)S(1)}, u32[]{:S(2)}, u32[]{:S(2)}) async-start(bf16[8,384,256]{2,1,0:T(8,128)(2,1)} %broadcast_in_dim.89), calls=%async_computation | async-start | bytes 3145728 | tf_op jit(solution)/shard_map/all_to_all | solution.py:28
  55.7 19.6 %all-to-all-done = bf16[8,384,256]{2,1,0:T(8,128)(2,1)S(1)} async-done(((bf16[8,384,256]{2,1,0:T(8,128)(2,1)}), bf16[8,384,256]{2,1,0:T(8,128)(2,1)S(1)}, u32[]{:S(2)}, u32[]{:S(2)}) %all-to-all-start) | async-done | bytes 1572896 | tf_op jit(solution)/shard_map/all_to_all | solution.py:28
  75.3 0.9 copy.96
  77.1 1.6 fusion.27
  78.6 97.4 %all-gather.4.cloned.1.call-done = bf16[2048,1152]{1,0:T(8,128)(2,1)} async-done(((bf16[64,1152]{1,0:T(8,128)(2,1)}), bf16[2048,1152]{1,0:T(8,128)(2,1)}) %all-gather.4.cloned.1.call-update) | async-done | bytes 4718608 | tf_op jit(solution)/shard_map/all_gather | solution.py:16
  176.0 2.3 slice_bitcast_fusion.2
  178.3 1.2 copy.108
  180.1 2.0 convolution_convert_fusion.1
  182.1 0.7 pad_maximum_fusion
  182.9 0.7 all-gather.8.cloned.1.call-update
  185.2 57.9 %all_gather.14 = f32[12288,2]{0,1:T(2,128)} all-gather(f32[384,2]{0,1:T(2,128)S(1)} %copy-done.3), channel_id=1, replica_groups=mesh['grp'=2,'sp'=32,'tp'=8] {'sp'}, dimensions={0}, use_global_device_ids=true | all-gather | bytes 101376 | tf_op jit(solution)/shard_map/all_gather | solution.py:100
  243.2 2.2 convolution_convert_fusion.2
  246.0 3.2 collective-permute-start
  249.3 1.9 multiply_reduce_fusion.4
  252.0 2.0 collective-permute-start.1
  254.7 0.7 multiply_convert_fusion.3
  255.4 1.3 multiply_convert_fusion.1
  257.3 0.9 fusion.72
  259.5 0.9 fusion.73
  261.5 60.5 %all-gather.6.cloned.1.call-done = bf16[12288,4,64]{0,2,1:T(8,128)(2,1)} async-done(((bf16[384,4,64]{0,2,1:T(8,128)(2,1)}), bf16[12288,4,64]{0,2,1:T(8,128)(2,1)}) %all-gather.6.cloned.1.call-update) | async-done | bytes 6291472 | tf_op jit(solution)/shard_map/all_gather | solution.py:16
  322.0 72.8 %conditional.1 = (f32[2,384]{1,0:T(2,128)}, f32[384,2,64]{0,2,1:T(8,128)}) conditional(s32[]{:T(128)} %bitcast.26, () %tuple.20, (bf16[12288,4,64]{0,2,1:T(8,128)(2,1)}, f32[12288,2]{0,1:T(2,128)}, s32[6,2048]{1,0:T(8,128)S(1)}, s32[6,2048]{1,0:T(8,128)S(1)}, s32[384]{0:T(512)S(1)}, /*index=5*/bf16[384,2,64]{0,2,1:T(8,128)(2,1)}, ...), branch_computations={%region_7.8_spmd, %region_8.13_spmd} | conditional | flops 430354944 | bytes 49433404 | solution.py:161
  322.3 3.3 fusion.78
  325.5 2.6 copy_bitcast_fusion
  328.1 66.7 %while.18 = (s32[]{:T(128)}, f32[2,384]{1,0:T(2,128)S(1)}, f32[2,384]{1,0:T(2,128)}, f32[384,2,64]{0,2,1:T(8,128)}, s32[384]{0:T(512)S(1)}, /*index=5*/s32[6,204...) while((s32[]{:T(128)}, f32[2,384]{1,0:T(2,128)S(1)}, ...), condition=%wide.region_12.12_spmd.clone, body=%wide.region_9.11_spmd.clone.sunk | while | flops 430330368 | bytes 23726752 | solution.py:156
  328.1 0.7 dynamic-slice_bitcast_fusion.2
  329.5 3.1 fusion.105
  332.6 2.0 fusion.107
  334.5 2.8 fusion.109
  337.9 0.7 dynamic-slice_bitcast_fusion.2
  339.2 3.1 fusion.105
  342.3 2.0 fusion.107
  344.3 3.7 fusion.109
  348.0 1.3 fusion.108
  349.3 0.7 dynamic-slice_bitcast_fusion.2
  350.6 3.1 fusion.105
  353.7 2.0 fusion.107
  355.7 3.7 fusion.109
  359.4 1.3 fusion.108
  360.7 0.7 dynamic-slice_bitcast_fusion.2
  362.0 3.1 fusion.105
  365.1 2.0 fusion.107
  367.0 3.7 fusion.109
  370.7 1.3 fusion.108
  372.1 0.7 dynamic-slice_bitcast_fusion.2
  373.4 3.1 fusion.105
  376.5 2.0 fusion.107
  378.4 3.7 fusion.109
  382.1 1.3 fusion.108
  383.4 0.7 dynamic-slice_bitcast_fusion.2
  384.7 3.1 fusion.105
  387.8 2.0 fusion.107
  389.8 3.7 fusion.109
  393.5 1.3 fusion.108
  394.8 1.1 divide_convert_fusion.2
  396.0 1.5 broadcast_in_dim.93
  397.5 4.6 all-to-all-start.1
  402.1 3.7 fusion.47
  405.7 1.6 reshape.322
  408.0 41.3 %all-gather.8.cloned.1.call-done = bf16[2,1024,256]{2,1,0:T(8,128)(2,1)} async-done(((bf16[2,32,256]{2,1,0:T(8,128)(2,1)}), bf16[2,1024,256]{2,1,0:T(8,128)(2,1)}) %all-gather.8.cloned.1.call-update) | async-done | bytes 1048592 | tf_op jit(solution)/shard_map/all_gather | solution.py:237
  449.3 1.8 fusion.39
  451.1 0.8 fusion.59
  (104 shorter events, 12.9 us)
Async XLA Ops:
  6.5 48.6 %copy-start.5 = (f32[2048]{0:T(1024)S(1)}, f32[2048]{0:T(1024)}, u32[]{:S(2)}) copy-start(f32[2048]{0:T(1024)} %param.18) | copy-start | bytes 24580
  6.5 48.6 %copy-start.7 = (f32[4,64]{1,0:T(4,128)S(1)}, f32[4,64]{1,0:T(4,128)}, u32[]{:S(2)}) copy-start(f32[4,64]{1,0:T(4,128)} %param.19) | copy-start | bytes 3076
  6.6 169.4 %all-gather.4.cloned.1.call-start = ((), (), s32[]{:S(2)}) async-start(), calls=%async_computation.2 | async-start | bytes 4866048 | tf_op jit(solution)/shard_map/all_gather | solution.py:16
  11.2 64.1 %all-to-all-start = ((bf16[8,384,256]{2,1,0:T(8,128)(2,1)}), bf16[8,384,256]{2,1,0:T(8,128)(2,1)S(1)}, u32[]{:S(2)}, u32[]{:S(2)}) async-start(bf16[8,384,256]{2,1,0:T(8,128)(2,1)} %broadcast_in_dim.89), calls=%async_computation | async-start | bytes 3145728 | tf_op jit(solution)/shard_map/all_to_all | solution.py:28
  55.2 266.8 %all-gather.6.cloned.1.call-start = ((), (), s32[]{:S(2)}) async-start(), calls=%async_computation.3 | async-start | bytes 6488064 | tf_op jit(solution)/shard_map/all_gather | solution.py:16
  179.5 5.7 %copy-start.3 = (f32[384,2]{0,1:T(2,128)S(1)}, f32[384,2]{0,1:T(2,128)}, u32[]{:S(2)}) copy-start(f32[384,2]{0,1:T(2,128)} %param.27) | copy-start | bytes 9220
  182.9 266.4 %all-gather.8.cloned.1.call-start = ((), (), s32[]{:S(2)}) async-start(), calls=%async_computation.4 | async-start | bytes 1081344 | tf_op jit(solution)/shard_map/all_gather | solution.py:237
  245.4 5.8 %copy-start.1 = (bf16[384,64]{0,1:T(8,128)(2,1)}, bf16[384,64]{0,1:T(8,128)(2,1)S(1)}, u32[]{:S(2)}) copy-start(bf16[384,64]{0,1:T(8,128)(2,1)S(1)} %convolution_convert_fusion.2) | copy-start | bytes 147460
  246.0 13.5 %collective-permute-start = (bf16[128,1,64]{0,2,1:T(8,128)(2,1)}, bf16[128,1,64]{0,2,1:T(8,128)(2,1)}, u32[]{:S(2)}, u32[]{:S(2)}) collective-permute-start(bf16[128,1,64]{0,2,1:T(8,128)(2,1)} %slice_bitcast_fusion.4), channel_id=1, source_target_pairs={{0,8},{8,16},{16,24},{24,32},{32,40},{40,48},{48,56},{56,64},{64,7... | collective-permute-start | bytes 49160 | tf_op jit(solution)/shard_map/ppermute | solution.py:40
  251.9 5.1 %copy-start.2 = (bf16[384,64]{0,1:T(8,128)(2,1)S(1)}, bf16[384,64]{0,1:T(8,128)(2,1)}, u32[]{:S(2)}) copy-start(bf16[384,64]{0,1:T(8,128)(2,1)} %copy-done.1) | copy-start | bytes 147460
  252.0 5.3 %collective-permute-start.1 = (bf16[128,1,64]{0,2,1:T(8,128)(2,1)S(1)}, bf16[128,1,64]{0,2,1:T(8,128)(2,1)}, u32[]{:S(2)}, u32[]{:S(2)}) collective-permute-start(bf16[128,1,64]{0,2,1:T(8,128)(2,1)S(1)} %slice_bitcast_fusion.3), channel_id=1, source_target_pairs={{0,8},{8,16},{16,24},{24,32},{32,40},{40,48},{48,56},{56,64},{64,7... | collective-permute-start | bytes 49160 | tf_op jit(solution)/shard_map/ppermute | solution.py:40
  254.2 4.8 %copy-start.6 = (f32[2]{0:T(128)S(1)}, f32[2]{0:T(128)}, u32[]{:S(2)}) copy-start(f32[2]{0:T(128)} %param.23) | copy-start | bytes 28
  325.5 2.6 copy-start.4
  394.8 7.3 %copy-start = (bf16[384,2048]{0,1:T(8,128)(2,1)S(1)}, bf16[384,2048]{0,1:T(8,128)(2,1)}, u32[]{:S(2)}) copy-start(bf16[384,2048]{0,1:T(8,128)(2,1)} %fusion.27) | copy-start | bytes 4718596
  397.5 51.8 %all-to-all-start.1 = ((bf16[8,384,2,128]{3,1,2,0:T(8,128)(2,1)}), bf16[8,384,2,128]{3,1,2,0:T(8,128)(2,1)S(1)}, u32[]{:S(2)}, u32[]{:S(2)}) async-start(bf16[8,384,2,128]{3,1,2,0:T(8,128)(2,1)} %broadcast_in_dim.93), calls=%async_computation.1 | async-start | bytes 3145728 | tf_op jit(solution)/shard_map/all_to_all | solution.py:28
Sparse Core Ops, SparseCore 0:
  9.4 166.5 all-gather.3
  183.0 138.9 all-gather.5
  324.1 125.1 all-gather.7
where the time goes:
time: 460 us; the launch traced here: 458 us
  waiting for transfers between devices  220 us (48%)
  blocking collectives  57.9 us (13%)
  starting transfers between devices  53.8 us (12%)
  matrix products  53.5 us (12%)
  other arithmetic  32.1 us (7%)
  local copies, waits for them, and re-layouts  26.7 us (6%)
  between operations  14.3 us (3%)
    all_gather x2, waiting for transfers between devices, sent_together(): filled = lax.all_gather(both, axis, axis=dim, tiled=True)  158 us
    all_gather x1, blocking collectives, forget_groups(): gates_all = lax.all_gather(gates, 'sp', axis=0, tiled=True)  57.9 us
    all_to_all x2, starting transfers between devices, sent_to_all(): lax.all_to_all(jnp.broadcast_to(value[None], (size, *value.shape)), axis,...  48.5 us
    all_gather x1, waiting for transfers between devices, on_device(): branch_full = lax.all_gather(w_branch, 'sp', axis=1, tiled=True)  41.3 us
    dot_general x6, matrix products, absorb(): jnp.einsum('hqk,khd->qhd', weights.astype(jnp.bfloat16), value_rows, pref...  21.3 us
    all_to_all x2, waiting for transfers between devices, sent_to_all(): lax.all_to_all(jnp.broadcast_to(value[None], (size, *value.shape)), axis,...  19.6 us
    dot_general x6, matrix products, absorb(): jnp.einsum('qhd,khd->hqk', queries, key_rows, preferred_element_type=jnp....  18.4 us
    reduce_sum x6, other arithmetic, absorb(): row_total = row_total * shrink + jnp.sum(weights, axis=-1)  11.8 us
  transfers between devices with their start and end apart: 7, of which 4 were waited for; matrix products, arithmetic and copies ran while one was open for 22% of the time, Pallas kernels for 0%

commit v1 on v0

--- a/solution.py
+++ b/solution.py
@@ -234,7 +234,9 @@
     )[0]
     channel_count = w_merge.shape[2]
     merge_gate = jax.nn.sigmoid(projected[6]).reshape(row_count, 2, channel_count)
-    branch_full = lax.all_gather(w_branch, "sp", axis=1, tiled=True)
+    branch_full = jnp.concatenate(
+        lax.all_to_all(jnp.stack([w_branch] * lax.axis_size("sp")), "sp", 0, 0), axis=1
+    )
     head_stack = jnp.stack([window_out, forget_out], axis=1)
     weight_rows = branch_full
     projection = jnp.einsum(

time: 460 us -> 492 us (1.070)
  the two profiles are of different devices: /device:TPU:34 before, /device:TPU:33 now
where the time goes in v1:
time: 492 us; the launch traced here: 490 us
  waiting for transfers between devices  153 us (31%)
  blocking collectives  123 us (25%)
  starting transfers between devices  85 us (17%)
  matrix products  55.6 us (11%)
  other arithmetic  31.5 us (6%)
  local copies, waits for them, and re-layouts  26.7 us (5%)
  between operations  14.5 us (3%)
    all_gather x1, blocking collectives, forget_groups(): gates_all = lax.all_gather(gates, 'sp', axis=0, tiled=True)  123 us
    all_gather x2, waiting for transfers between devices, sent_together(): filled = lax.all_gather(both, axis, axis=dim, tiled=True)  117 us
    all_to_all x2, starting transfers between devices, sent_to_all(): lax.all_to_all(jnp.broadcast_to(value[None], (size, *value.shape)), axis,...  67.4 us
    all_to_all x2, waiting for transfers between devices, sent_to_all(): lax.all_to_all(jnp.broadcast_to(value[None], (size, *value.shape)), axis,...  35.8 us
    dot_general x6, matrix products, absorb(): jnp.einsum('hqk,khd->qhd', weights.astype(jnp.bfloat16), value_rows, pref...  23.1 us
    dot_general x6, matrix products, absorb(): jnp.einsum('qhd,khd->hqk', queries, key_rows, preferred_element_type=jnp....  18.4 us
    all_to_all x1, starting transfers between devices, on_device(): lax.all_to_all(jnp.stack([w_branch] * lax.axis_size('sp')), 'sp', 0, 0)  12.4 us
    reduce_sum x6, other arithmetic, absorb(): row_total = row_total * shrink + jnp.sum(weights, axis=-1)  11.8 us
  transfers between devices with their start and end apart: 7, of which 4 were waited for; matrix products, arithmetic and copies ran while one was open for 21% of the time, Pallas kernels for 0%

profile of v1, /device:TPU:33, one launch (start us, length us, event | category | flops | bytes accessed | tf_op | source)
XLA Modules:
  0.0 490.2 jit_solution(17491918878885817620)
XLA Ops:
  6.6 0.9 copy.131
  7.4 1.6 concatenate.18
  9.0 2.2 broadcast_in_dim.89
  11.2 44.9 %all-to-all-start = ((bf16[8,384,256]{2,1,0:T(8,128)(2,1)}), bf16[8,384,256]{2,1,0:T(8,128)(2,1)S(1)}, u32[]{:S(2)}, u32[]{:S(2)}) async-start(bf16[8,384,256]{2,1,0:T(8,128)(2,1)} %broadcast_in_dim.89), calls=%async_computation | async-start | bytes 3145728 | tf_op jit(solution)/shard_map/all_to_all | solution.py:28
  56.8 20.1 %all-to-all-done = bf16[8,384,256]{2,1,0:T(8,128)(2,1)S(1)} async-done(((bf16[8,384,256]{2,1,0:T(8,128)(2,1)}), bf16[8,384,256]{2,1,0:T(8,128)(2,1)S(1)}, u32[]{:S(2)}, u32[]{:S(2)}) %all-to-all-start) | async-done | bytes 1572896 | tf_op jit(solution)/shard_map/all_to_all | solution.py:28
  76.8 0.9 copy.97
  78.5 1.6 fusion.27
  80.1 77.1 %all-gather.3.cloned.1.call-done = bf16[2048,1152]{1,0:T(8,128)(2,1)} async-done(((bf16[64,1152]{1,0:T(8,128)(2,1)}), bf16[2048,1152]{1,0:T(8,128)(2,1)}) %all-gather.3.cloned.1.call-update) | async-done | bytes 4718608 | tf_op jit(solution)/shard_map/all_gather | solution.py:16
  157.3 2.5 slice_bitcast_fusion.2
  160.5 2.0 convolution_convert_fusion.1
  162.5 0.7 pad_maximum_fusion
  163.3 1.1 stack.5
  164.4 12.4 %all-to-all-start.2 = ((bf16[32,2,32,256]{3,2,1,0:T(8,128)(2,1)}), bf16[32,2,32,256]{3,2,1,0:T(8,128)(2,1)S(1)}, u32[]{:S(2)}, u32[]{:S(2)}) async-start(bf16[32,2,32,256]{3,2,1,0:T(8,128)(2,1)} %stack.5), calls=%async_computation.2 | async-start | bytes 2097152 | tf_op jit(solution)/shard_map/all_to_all | solution.py:238
  176.8 0.7 slice.62
  178.2 123.1 %all_gather.11 = f32[12288,2]{0,1:T(2,128)S(1)} all-gather(f32[384,2]{0,1:T(2,128)S(1)} %copy-done.2), channel_id=1, replica_groups=mesh['grp'=2,'sp'=32,'tp'=8] {'sp'}, dimensions={0}, use_global_device_ids=true | all-gather | bytes 101376 | tf_op jit(solution)/shard_map/all_gather | solution.py:100
  301.5 2.2 convolution_convert_fusion.2
  304.3 3.3 collective-permute-start
  307.6 1.3 copy.105
  308.8 1.9 multiply_reduce_fusion.4
  311.5 1.9 collective-permute-start.1
  313.4 2.0 copy.111
  315.9 1.5 multiply_reduce_fusion.1
  317.4 0.7 multiply_convert_fusion.3
  318.1 0.8 multiply_convert_fusion.1
  319.5 0.9 fusion.73
  320.5 0.9 fusion.72
  323.7 40.2 %all-gather.5.cloned.1.call-done = bf16[12288,4,64]{0,2,1:T(8,128)(2,1)} async-done(((bf16[384,4,64]{0,2,1:T(8,128)(2,1)}), bf16[12288,4,64]{0,2,1:T(8,128)(2,1)}) %all-gather.5.cloned.1.call-update) | async-done | bytes 6291472 | tf_op jit(solution)/shard_map/all_gather | solution.py:16
  363.9 70.9 %conditional.1 = (f32[2,384]{1,0:T(2,128)}, f32[384,2,64]{0,2,1:T(8,128)}) conditional(s32[]{:T(128)} %bitcast.26, () %tuple.20, (bf16[12288,4,64]{0,2,1:T(8,128)(2,1)}, f32[12288,2]{0,1:T(2,128)S(1)}, s32[6,2048]{1,0:T(8,128)S(1)}, s32[6,2048]{1,0:T(8,128)S(1)}, s32[384]{0:T(512)S(1)}, /*index=5*/bf16[384,2,64]{0,2,1:T(8,128)(2,1)S(1)}, ...), branch_computations={%region_7.8_spmd, %region_8.13_spmd} | conditional | flops 430354944 | bytes 49040160 | solution.py:161
  364.2 3.3 fusion.78
  367.4 3.2 copy_bitcast_fusion
  370.6 64.2 %while.18 = (s32[]{:T(128)}, f32[2,384]{1,0:T(2,128)S(1)}, f32[2,384]{1,0:T(2,128)}, f32[384,2,64]{0,2,1:T(8,128)}, s32[384]{0:T(512)S(1)}, /*index=5*/s32[6,204...) while((s32[]{:T(128)}, f32[2,384]{1,0:T(2,128)S(1)}, ...), condition=%wide.region_12.12_spmd.clone, body=%wide.region_9.11_spmd.clone.sunk | while | flops 430330368 | bytes 23726752 | solution.py:156
  371.3 3.1 fusion.105
  374.4 2.0 fusion.107
  376.3 3.8 fusion.109
  380.1 0.6 fusion.108
  381.4 3.1 fusion.105
  384.5 2.0 fusion.107
  386.4 3.9 fusion.109
  390.3 1.3 fusion.108
  392.2 3.1 fusion.105
  395.3 2.0 fusion.107
  397.2 3.9 fusion.109
  401.1 1.3 fusion.108
  403.0 3.1 fusion.105
  406.1 2.0 fusion.107
  408.1 3.9 fusion.109
  411.9 1.3 fusion.108
  413.8 3.1 fusion.105
  416.9 2.0 fusion.107
  418.9 3.9 fusion.109
  422.7 1.3 fusion.108
  424.6 3.1 fusion.105
  427.7 2.0 fusion.107
  429.7 3.9 fusion.109
  433.6 1.3 fusion.108
  434.8 0.9 divide_convert_fusion.2
  436.0 1.5 broadcast_in_dim.93
  437.4 22.5 %all-to-all-start.1 = ((bf16[8,384,2,128]{3,1,2,0:T(8,128)(2,1)}), bf16[8,384,2,128]{3,1,2,0:T(8,128)(2,1)}, u32[]{:S(2)}, u32[]{:S(2)}) async-start(bf16[8,384,2,128]{3,1,2,0:T(8,128)(2,1)} %broadcast_in_dim.93), calls=%async_computation.1 | async-start | bytes 3145728 | tf_op jit(solution)/shard_map/all_to_all | solution.py:28
  459.9 1.1 copy.115
  461.0 2.7 fusion.47
  464.2 0.6 fusion.79
  464.8 15.8 %all-to-all-done.1 = bf16[8,384,2,128]{3,1,2,0:T(8,128)(2,1)} async-done(((bf16[8,384,2,128]{3,1,2,0:T(8,128)(2,1)}), bf16[8,384,2,128]{3,1,2,0:T(8,128)(2,1)}, u32[]{:S(2)}, u32[]{:S(2)}) %all-to-all-start.1) | async-done | bytes 1572896 | tf_op jit(solution)/shard_map/all_to_all | solution.py:28
  480.6 2.0 fusion.39
  482.6 0.8 fusion.59
  (103 shorter events, 11.6 us)
Async XLA Ops:
  6.5 49.6 %copy-start.3 = (f32[2048]{0:T(1024)S(1)}, f32[2048]{0:T(1024)}, u32[]{:S(2)}) copy-start(f32[2048]{0:T(1024)} %param.18) | copy-start | bytes 24580
  6.5 49.6 %copy-start.6 = (f32[4,64]{1,0:T(4,128)S(1)}, f32[4,64]{1,0:T(4,128)}, u32[]{:S(2)}) copy-start(f32[4,64]{1,0:T(4,128)} %param.19) | copy-start | bytes 3076
  6.6 150.7 %all-gather.3.cloned.1.call-start = ((), (), s32[]{:S(2)}) async-start(), calls=%async_computation.3 | async-start | bytes 4866048 | tf_op jit(solution)/shard_map/all_gather | solution.py:16
  11.2 65.6 %all-to-all-start = ((bf16[8,384,256]{2,1,0:T(8,128)(2,1)}), bf16[8,384,256]{2,1,0:T(8,128)(2,1)S(1)}, u32[]{:S(2)}, u32[]{:S(2)}) async-start(bf16[8,384,256]{2,1,0:T(8,128)(2,1)} %broadcast_in_dim.89), calls=%async_computation | async-start | bytes 3145728 | tf_op jit(solution)/shard_map/all_to_all | solution.py:28
  56.2 307.8 %all-gather.5.cloned.1.call-start = ((), (), s32[]{:S(2)}) async-start(), calls=%async_computation.4 | async-start | bytes 6488064 | tf_op jit(solution)/shard_map/all_gather | solution.py:16
  159.9 3.4 copy-start.4
  160.5 17.7 %copy-start.2 = (f32[384,2]{0,1:T(2,128)S(1)}, f32[384,2]{0,1:T(2,128)}, u32[]{:S(2)}) copy-start(f32[384,2]{0,1:T(2,128)} %param.27) | copy-start | bytes 9220
  164.4 271.5 %all-to-all-start.2 = ((bf16[32,2,32,256]{3,2,1,0:T(8,128)(2,1)}), bf16[32,2,32,256]{3,2,1,0:T(8,128)(2,1)S(1)}, u32[]{:S(2)}, u32[]{:S(2)}) async-start(bf16[32,2,32,256]{3,2,1,0:T(8,128)(2,1)} %stack.5), calls=%async_computation.2 | async-start | bytes 2097152 | tf_op jit(solution)/shard_map/all_to_all | solution.py:238
  304.3 15.2 %collective-permute-start = (bf16[128,1,64]{0,2,1:T(8,128)(2,1)}, bf16[128,1,64]{0,2,1:T(8,128)(2,1)}, u32[]{:S(2)}, u32[]{:S(2)}) collective-permute-start(bf16[128,1,64]{0,2,1:T(8,128)(2,1)} %slice_bitcast_fusion.4), channel_id=1, source_target_pairs={{0,8},{8,16},{16,24},{24,32},{32,40},{40,48},{48,56},{56,64},{64,7... | collective-permute-start | bytes 49160 | tf_op jit(solution)/shard_map/ppermute | solution.py:40
  311.5 9.1 %collective-permute-start.1 = (bf16[128,1,64]{0,2,1:T(8,128)(2,1)}, bf16[128,1,64]{0,2,1:T(8,128)(2,1)}, u32[]{:S(2)}, u32[]{:S(2)}) collective-permute-start(bf16[128,1,64]{0,2,1:T(8,128)(2,1)} %slice_bitcast_fusion.3), channel_id=1, source_target_pairs={{0,8},{8,16},{16,24},{24,32},{32,40},{40,48},{48,56},{56,64},{64,7... | collective-permute-start | bytes 49160 | tf_op jit(solution)/shard_map/ppermute | solution.py:40
  317.4 5.0 %copy-start.5 = (f32[2]{0:T(128)S(1)}, f32[2]{0:T(128)}, u32[]{:S(2)}) copy-start(f32[2]{0:T(128)} %param.23) | copy-start | bytes 28
  435.9 25.0 %copy-start = (bf16[384,2048]{0,1:T(8,128)(2,1)S(1)}, bf16[384,2048]{0,1:T(8,128)(2,1)}, u32[]{:S(2)}) copy-start(bf16[384,2048]{0,1:T(8,128)(2,1)} %fusion.27) | copy-start | bytes 4718596
  437.4 43.2 %all-to-all-start.1 = ((bf16[8,384,2,128]{3,1,2,0:T(8,128)(2,1)}), bf16[8,384,2,128]{3,1,2,0:T(8,128)(2,1)}, u32[]{:S(2)}, u32[]{:S(2)}) async-start(bf16[8,384,2,128]{3,1,2,0:T(8,128)(2,1)} %broadcast_in_dim.93), calls=%async_computation.1 | async-start | bytes 3145728 | tf_op jit(solution)/shard_map/all_to_all | solution.py:28
  463.7 16.9 %copy-start.1 = (bf16[2,32,32,256]{3,2,1,0:T(8,128)(2,1)S(1)}, bf16[2,32,32,256]{3,2,1,0:T(8,128)(2,1)}, u32[]{:S(2)}) copy-start(bf16[2,32,32,256]{3,2,1,0:T(8,128)(2,1)} %copy.115) | copy-start | bytes 3145732
Sparse Core Ops, SparseCore 0:
  9.4 147.7 all-gather.2
  163.4 200.4 all-gather.4
